TPU v7x, 32 devices: a whole 2x2x4 slice. The times are simulated.
32 devices in a mesh: grp: 2 (over y), kv: 4 (over z), tp: 4 (over x, core).
Axes of the slice: x: 2, y: 2, z: 4, core: 2. Of those that a mesh axis runs over, the one named last changes fastest.
Arguments:
- tokens: bfloat16 [16, 4096], P('grp', 'kv'), parts along dimension 0, may hold values from -6 to 6
- norm_gain: float32 [4096], replicated, may hold values from 0.1 to 1.9
- w_query: bfloat16 [4096, 4096], P('kv', 'tp'), may hold values from -0.09375 to 0.09375
- key_weight: bfloat16 [4096, 512], P('kv', 'tp'), may hold values from -0.09375 to 0.09375
- value_weight: bfloat16 [4096, 512], P('kv', 'tp'), may hold values from -0.09375 to 0.09375
- w_gate: bfloat16 [4096, 64], replicated, may hold values from -0.09375 to 0.09375
- gate_bias: float32 [64], replicated, may hold values from -3 to 4
- w_out: bfloat16 [4096, 4096], P('kv', 'tp'), may hold values from -0.1875 to 0.1875
- cache_keys: bfloat16 [16, 3072, 512], P('grp', 'kv', 'tp'), parts along dimension 0, may hold values from -240 to 240
- cache_values: bfloat16 [16, 3072, 512], P('grp', 'kv', 'tp'), parts along dimension 0, may hold values from -8 to 8
- cache_gate: float32 [16, 64, 3072], P('grp', 'tp', 'kv'), parts along dimension 0, may hold values from -3072 to 0, as said below
- gate_total: float32 [16, 64], P('grp', 'tp'), parts along dimension 0, may hold values from -3072 to 0, as said below
- lengths: int32 [16], P('grp'), parts along dimension 0, may hold values from 1536 to 3072, as said below
Outputs:
- mixed: bfloat16 [16, 4096], P('grp', 'kv'), parts along dimension 0
- key_new: bfloat16 [16, 512], P('grp', 'tp'), parts along dimension 0
- value_new: bfloat16 [16, 512], P('grp', 'tp'), parts along dimension 0
There are 2 independent parts, one for each index of `grp`. A program takes and returns all parts, laid end to end along the dimension named above; an argument that names none is the same for every part. Nothing has to cross between parts.
Inputs may be any that keep to these rules, and one draw needn't show every extreme that they name: `lengths`: one sequence of each draw has all 3072 positions cached. `cache_gate`: non-increasing along positions. `gate_total`: equal to cache_gate at position lengths - 1 of the same sequence and head.
All inputs are finite; a program needn't handle non-finite values.
Results may differ from a plain program's by a relative error of at most 0.015.
Values may be sent and summed in bfloat16 or wider, within the bound.
A program may use at most 64 MiB of HBM per device.

v0:
```python
import jax
import jax.numpy as jnp
from jax import lax
from jax.sharding import PartitionSpec as P

HEAD_SIZE = 64
NEG_FILL = -1e30


def per_device(
    tokens,
    norm_gain,
    w_query,
    key_weight,
    value_weight,
    w_gate,
    gate_bias,
    w_out,
    cache_keys,
    cache_values,
    cache_gate,
    gate_total,
    lengths,
):
    seq_count = tokens.shape[0]
    width_dev = tokens.shape[1]
    heads_dev = cache_gate.shape[1]
    positions_dev = cache_gate.shape[2]
    kv_heads_dev = cache_keys.shape[2] // HEAD_SIZE
    head_group = heads_dev // kv_heads_dev
    logit_scale = HEAD_SIZE ** (-0.5)
    whole = lax.all_gather(tokens, "kv", axis=1, tiled=True)
    features = whole.astype(jnp.float32)
    normed = (
        features
        * lax.rsqrt(jnp.mean(features * features, axis=-1, keepdims=True) + 1e-06)
        * norm_gain
    )
    normed = normed.astype(jnp.bfloat16)
    kv_index = lax.axis_index("kv")
    tp_index = lax.axis_index("tp")
    own_rows = lax.dynamic_slice_in_dim(normed, kv_index * width_dev, width_dev, 1)
    query_part = jnp.dot(own_rows, w_query, preferred_element_type=jnp.float32)
    key_part = jnp.dot(own_rows, key_weight, preferred_element_type=jnp.float32)
    value_part = jnp.dot(own_rows, value_weight, preferred_element_type=jnp.float32)
    query_sum, key_sum, value_sum = lax.psum((query_part, key_part, value_part), "kv")
    query = query_sum.astype(jnp.bfloat16)
    key_new = key_sum.astype(jnp.bfloat16)
    value_new = value_sum.astype(jnp.bfloat16)
    gate_cols = lax.dynamic_slice_in_dim(w_gate, tp_index * heads_dev, heads_dev, 1)
    bias_cols = lax.dynamic_slice_in_dim(gate_bias, tp_index * heads_dev, heads_dev, 0)
    log_gate = jax.nn.log_sigmoid(
        jnp.dot(normed, gate_cols, preferred_element_type=jnp.float32) + bias_cols
    )
    level = gate_total + log_gate
    query_head_rows = query.reshape(seq_count, kv_heads_dev, head_group, HEAD_SIZE)
    key_block = cache_keys.reshape(seq_count, positions_dev, kv_heads_dev, HEAD_SIZE)
    value_block = cache_values.reshape(seq_count, positions_dev, kv_heads_dev, HEAD_SIZE)
    score_matrix = (
        jnp.einsum(
            "skgd,spkd->skgp", query_head_rows, key_block, preferred_element_type=jnp.float32
        )
        * logit_scale
    )
    forget_bias = (level[:, :, None] - cache_gate).reshape(
        seq_count, kv_heads_dev, head_group, positions_dev
    )
    positions = kv_index * positions_dev + jnp.arange(positions_dev, dtype=jnp.int32)
    valid_mask = (positions[None, :] < lengths[:, None])[:, None, None, :]
    score_matrix = jnp.where(valid_mask, score_matrix + forget_bias, NEG_FILL)
    local_max = jnp.max(score_matrix, axis=-1)
    weights = jnp.where(valid_mask, jnp.exp(score_matrix - local_max[..., None]), 0.0)
    local_total = jnp.sum(weights, axis=-1)
    local_values = jnp.einsum(
        "skgp,spkd->skgd",
        weights.astype(jnp.bfloat16),
        value_block,
        preferred_element_type=jnp.float32,
    )
    block_max = lax.pmax(local_max, "kv")
    rescale = jnp.exp(local_max - block_max)
    block_total, block_values = lax.psum(
        (local_total * rescale, local_values * rescale[..., None]), "kv"
    )
    key_current = key_new.reshape(seq_count, kv_heads_dev, HEAD_SIZE)
    current_score = (
        jnp.einsum(
            "skgd,skd->skg", query_head_rows, key_current, preferred_element_type=jnp.float32
        )
        * logit_scale
    )
    top = jnp.maximum(block_max, current_score)
    cached_scale = jnp.exp(block_max - top)
    current_weight = jnp.exp(current_score - top)
    denominator = block_total * cached_scale + current_weight
    value_current = value_new.reshape(seq_count, kv_heads_dev, 1, HEAD_SIZE).astype(jnp.float32)
    total_sum = block_values * cached_scale[..., None] + current_weight[..., None] * value_current
    attended = (
        (total_sum / denominator[..., None])
        .reshape(seq_count, heads_dev * HEAD_SIZE)
        .astype(jnp.bfloat16)
    )
    partial_value = lax.dot_general(
        attended, w_out, (((1,), (1,)), ((), ())), preferred_element_type=jnp.float32
    )
    partial_value = lax.optimization_barrier(partial_value.astype(jnp.bfloat16)).astype(jnp.float32)
    mixed = lax.psum(partial_value.astype(jnp.bfloat16), "tp")
    return (mixed, key_new, value_new)


def solution(mesh):
    placed = (
        P("grp", "kv"),
        P(),
        P("kv", "tp"),
        P("kv", "tp"),
        P("kv", "tp"),
        P(),
        P(),
        P("kv", "tp"),
        P("grp", "kv", "tp"),
        P("grp", "kv", "tp"),
        P("grp", "tp", "kv"),
        P("grp", "tp"),
        P("grp"),
    )
    return jax.shard_map(
        per_device,
        mesh=mesh,
        in_specs=placed,
        out_specs=(P("grp", "kv"), P("grp", "tp"), P("grp", "tp")),
        check_vma=False,
    )
```

profile of v0, /device:TPU:0, one launch (start us, length us, event | category | flops | bytes accessed | tf_op | source)
XLA Modules:
  0.0 91.3 jit_solution(11908319094124294041)
XLA Ops:
  0.7 0.9 dynamic_slice.11
  1.5 0.7 broadcast_compare_fusion
  2.3 15.1 %all_gather.3 = bf16[8,4096]{1,0:T(8,128)(2,1)S(1)} all-gather(bf16[8,1024]{1,0:T(8,128)(2,1)} %param.13), channel_id=1, replica_groups=mesh['grp'=2,'kv'=4,'tp'=4] {'kv'}, dimensions={1}, use_global_device_ids=true | all-gather | bytes 81920 | tf_op jit(solution)/shard_map/all_gather | solution.py:32
  17.4 0.1 fusion.9
  17.5 0.8 fusion.11
  18.4 1.1 %fusion.22 = f32[8,16]{1,0:T(8,128)S(1)} fusion(f32[8,16]{1,0:T(8,128)} %param.24, bf16[8,4096]{1,0:T(8,128)(2,1)S(1)} %fusion.11, bf16[4096,64]{0,1:T(8,128)(2,1)} %param.18, s32[]{:T(128)S(6)} %select_n.20, f32[16]{0:T(128)S(1)} %dynamic_slice.11), kind=kOutput, calls=%fused_computation.35 | convolution fusion | flops 1049856 | bytes 201284 | tf_op jit(solution)/shard_map/dot_general | solution.py:53
  19.4 1.1 %fusion.15 = f32[8,128]{1,0:T(8,128)S(1)} fusion(bf16[1024,128]{1,0:T(8,128)(2,1)} %param.16, bf16[8,4096]{1,0:T(8,128)(2,1)S(1)} %fusion.11, s32[]{:T(128)S(6)} %select_n.19), kind=kOutput, calls=%fused_computation.24 | convolution fusion | flops 2097152 | bytes 282628 | tf_op jit(solution)/shard_map/dot_general | solution.py:44
  20.6 1.1 %fusion.13 = f32[8,128]{1,0:T(8,128)S(1)} fusion(bf16[1024,128]{1,0:T(8,128)(2,1)} %param.17, bf16[8,4096]{1,0:T(8,128)(2,1)S(1)} %fusion.11, s32[]{:T(128)S(6)} %select_n.19), kind=kOutput, calls=%fused_computation.22 | convolution fusion | flops 2097152 | bytes 282628 | tf_op jit(solution)/shard_map/dot_general | solution.py:45
  21.7 0.4 fusion.17
  22.0 19.1 %psum.42 = bf16[8,1024]{1,0:T(8,128)(2,1)S(1)} all-reduce(f32[8,1024]{1,0:T(8,128)S(1)} %fusion.17), channel_id=1, replica_groups=mesh['grp'=2,'kv'=4,'tp'=4] {'kv'}, use_global_device_ids=true, to_apply=%region_1.0 | all-reduce | flops 8192 | bytes 49152 | tf_op jit(solution)/shard_map/psum | solution.py:46
  41.2 0.1 reshape.76
  41.3 2.7 %copy.18 = bf16[8,768,128]{1,2,0:T(8,128)(2,1)} copy(bf16[8,768,128]{2,1,0:T(8,128)(2,1)} %param.21) | data formatting | bytes 3145728 | tf_op args[8]
  43.9 1.8 %fusion.33 = (f32[8,2,8]{2,1,0:T(2,128)S(1)}, f32[8,2,8,768]{3,2,1,0:T(8,128)S(1)}) fusion(f32[8,16,768]{2,1,0:T(8,128)S(1)} %copy-done.1, f32[8,16]{1,0:T(8,128)S(1)} %fusion.22, bf16[8,2,8,64]{3,2,1,0:T(8,128)(2,1)S(1)} %reshape.76, bf16[8,768,2,64]{1,3,2,0:T(8,128)(2,1)} %bitcast.24, pred[8,768]{1,0:T(8,128)(4,1)S(1)} %broadcast_compare_fusion), kind=kOutput, calls=%fused_computation.44 | convolution fusion | flops 13074304 | bytes 2382848 | tf_op jit(solution)/shard_map/skgd,spkd->skgp/dot_general | solution.py:60
  45.7 8.5 %pmax.7 = f32[8,2,8]{2,1,0:T(2,128)S(1)} all-reduce(f32[8,2,8]{2,1,0:T(2,128)S(1)} %get-tuple-element.12), channel_id=1, replica_groups=mesh['grp'=2,'kv'=4,'tp'=4] {'kv'}, use_global_device_ids=true, to_apply=%region_3.0 | all-reduce | flops 128 | bytes 1024 | tf_op jit(solution)/shard_map/pmax | solution.py:80
  54.3 0.2 fusion.3
  54.5 2.6 %copy.19 = bf16[8,768,128]{1,2,0:T(8,128)(2,1)} copy(bf16[8,768,128]{2,1,0:T(8,128)(2,1)} %param.22) | data formatting | bytes 3145728 | tf_op args[9]
  57.1 2.0 %convolution_multiply_fusion.1 = f32[8,2,8,64]{3,2,1,0:T(8,128)S(1)} fusion(bf16[8,768,2,64]{1,3,2,0:T(8,128)(2,1)} %bitcast.25, f32[8,2,8,768]{3,2,1,0:T(8,128)S(1)} %get-tuple-element.13, f32[8,2,8]{2,1,0:T(2,128)S(1)} %get-tuple-element.12, pred[8,768]{1,0:T(8,128)(4,1)S(1)} %broadcast_compare_fusion, f32[8,2,8]{2,1,0:T(2,128)S(1)} %bitcast.30), kind=kOutput, calls=%fused_computation.3 | convolution fusion | flops 12886016 | bytes 2006016 | tf_op jit(solution)/shard_map/skgp,spkd->skgd/dot_general | solution.py:74
  59.1 18.7 %all-reduce = (f32[8,2,8,64]{3,2,1,0:T(8,128)S(1)}, bf16[8,128]{1,0:T(8,128)(2,1)S(1)}, f32[8,2,8]{2,1,0:T(2,128)S(1)}, bf16[8,128]{1,0:T(8,128)(2,1)S(1)}) all-reduce(f32[8,2,8,64]{3,2,1,0:T(8,128)S(1)} %convolution_multiply_fusion.1, f32[8,128]{1,0:T(8,128)S(1)} %fusion.15, ...), channel_id=1, replica_groups=mesh['grp'=2,'kv'=4,'tp'=4] {'kv'}, use_global_device_ids=true, to_apply=%region_4.5 | all-reduce | flops 10368 | bytes 78848 | tf_op jit(solution)/shard_map/psum | solution.py:82
  77.9 0.1 fusion.34
  78.1 0.1 reshape.81
  78.1 0.1 divide_convert_fusion
  78.3 0.1 convert_element_type.49
  78.4 2.2 %convolution_convert_fusion = bf16[8,1024]{1,0:T(8,128)(2,1)S(1)} fusion(bf16[8,1024]{1,0:T(8,128)(2,1)S(1)} %convert_element_type.49, bf16[1024,1024]{1,0:T(8,128)(2,1)} %param.20), kind=kOutput, calls=%fused_computation.4 | convolution fusion | flops 16785408 | bytes 2129920 | tf_op jit(solution)/shard_map/dot_general | solution.py:103
  80.6 10.7 %psum.47 = bf16[8,1024]{1,0:T(8,128)(2,1)} all-reduce(bf16[8,1024]{1,0:T(8,128)(2,1)S(1)} %convolution_convert_fusion), channel_id=1, replica_groups=mesh['grp'=2,'kv'=4,'tp'=4] {'tp'}, use_global_device_ids=true, to_apply=%region_9.10 | all-reduce | flops 8192 | bytes 32768 | tf_op jit(solution)/shard_map/psum | solution.py:107
  (13 shorter events, 0.2 us)
Async XLA Ops:
  0.6 21.0 %copy-start = (bf16[1024,1024]{1,0:T(8,128)(2,1)S(1)}, bf16[1024,1024]{1,0:T(8,128)(2,1)}, u32[]{:S(2)}) copy-start(bf16[1024,1024]{1,0:T(8,128)(2,1)} %param.15) | copy-start | bytes 6291460
  41.3 2.7 %copy-start.1 = (f32[8,16,768]{2,1,0:T(8,128)S(1)}, f32[8,16,768]{2,1,0:T(8,128)}, u32[]{:S(2)}) copy-start(f32[8,16,768]{2,1,0:T(8,128)} %param.23) | copy-start | bytes 1179652
  77.8 13.5 %copy-start.2 = (bf16[8,128]{1,0:T(8,128)(2,1)}, bf16[8,128]{1,0:T(8,128)(2,1)S(1)}, u32[]{:S(2)}) copy-start(bf16[8,128]{1,0:T(8,128)(2,1)S(1)} %get-tuple-element.4) | copy-start | bytes 6148
  77.8 13.5 %copy-start.3 = (bf16[8,128]{1,0:T(8,128)(2,1)}, bf16[8,128]{1,0:T(8,128)(2,1)S(1)}, u32[]{:S(2)}) copy-start(bf16[8,128]{1,0:T(8,128)(2,1)S(1)} %get-tuple-element.6) | copy-start | bytes 6148
where the time goes:
time: 91.8 us; the launch traced here: 91.3 us
  blocking collectives  72.2 us (79%)
  matrix products  9.82 us (11%)
  local copies, waits for them, and re-layouts  6.53 us (7%)
  other arithmetic  2.09 us (2%)
    psum x1, blocking collectives, per_device(): lax.psum((query_part, key_part, value_part), 'kv')  19.1 us
    psum x1, blocking collectives, per_device(): lax.psum((local_total * rescale, local_values * rescale[..., None]), 'kv')  18.7 us
    all_gather x1, blocking collectives, per_device(): whole = lax.all_gather(tokens, 'kv', axis=1, tiled=True)  15.1 us
    psum x1, blocking collectives, per_device(): mixed = lax.psum(partial_value.astype(jnp.bfloat16), 'tp')  10.7 us
    pmax x1, blocking collectives, per_device(): block_max = lax.pmax(local_max, 'kv')  8.5 us
    unnamed x10, local copies, waits for them, and re-layouts  5.29 us
    dot_general x1, matrix products, per_device(): lax.dot_general(attended, w_out, (((1,), (1,)), ((), ())), preferred_elem...  2.23 us
    dot_general x1, matrix products, per_device(): jnp.einsum('skgp,spkd->skgd', weights.astype(jnp.bfloat16), value_block,...  1.98 us

commit v1 on v0

--- a/solution.py
+++ b/solution.py
@@ -29,7 +29,18 @@
     kv_heads_dev = cache_keys.shape[2] // HEAD_SIZE
     head_group = heads_dev // kv_heads_dev
     logit_scale = HEAD_SIZE ** (-0.5)
-    whole = lax.all_gather(tokens, "kv", axis=1, tiled=True)
+    n_peers_all = lax.axis_size("kv")
+    history = []
+    for to_i in range(1, n_peers_all):
+        history.append((to_i - 1, to_i))
+    aux = history + [(n_peers_all - 1, 0)]
+    long_array = tokens
+    blocks_here = [long_array]
+    for _ in range(n_peers_all - 1):
+        long_array = lax.ppermute(long_array, "kv", aux)
+        blocks_here += [long_array]
+    out_arr = jnp.concatenate([*reversed(blocks_here)], 1)
+    whole = jnp.roll(out_arr, (lax.axis_index("kv") + 1) * long_array.shape[1], axis=1)
     features = whole.astype(jnp.float32)
     normed = (
         features

time: 91.8 us -> 86.3 us (0.940)
  blocking collectives: 72.2 us -> 57.4 us
  waiting for transfers between devices: 0 us -> 9.49 us
  starting transfers between devices: 0 us -> 3.11 us
  matrix products: 9.82 us -> 7.91 us
    all_gather x1 -> x0, blocking collectives: 15.1 us -> none  [per_device(): whole = lax.all_gather(tokens, 'kv', axis=1, tiled=True)]
    ppermute x0 -> x3, waiting for transfers between devices: none -> 9.49 us  [per_device(): long_array = lax.ppermute(long_array, 'kv', aux)]
    ppermute x0 -> x3, starting transfers between devices: none -> 3.11 us  [per_device(): long_array = lax.ppermute(long_array, 'kv', aux)]
    dot_general x1, matrix products: 1.11 us -> 0.15 us  [per_device(): key_part = jnp.dot(own_rows, key_weight, preferred_element_type=jnp.float32)]
    dot_general x1, matrix products: 1.1 us -> 0.15 us  [per_device(): jnp.dot(own_rows, value_weight, preferred_element_type=jnp.float32)]
    unnamed x10 -> x29, local copies, waits for them, and re-layouts: 5.29 us -> 5.34 us
  transfers between devices with their start and end apart: 0 -> 3, of which waited for: 0 -> 2; matrix products, arithmetic and copies ran while one was open for 0% -> 7% of each run, Pallas kernels for 0% -> 0%
where the time goes in v1:
time: 86.3 us; the launch traced here: 85.9 us
  blocking collectives  57.4 us (67%)
  waiting for transfers between devices  9.49 us (11%)
  matrix products  7.91 us (9%)
  local copies, waits for them, and re-layouts  5.77 us (7%)
  starting transfers between devices  3.11 us (4%)
  other arithmetic  1.38 us (2%)
    psum x1, blocking collectives, per_device(): lax.psum((query_part, key_part, value_part), 'kv')  19.5 us
    psum x1, blocking collectives, per_device(): lax.psum((local_total * rescale, local_values * rescale[..., None]), 'kv')  18.7 us
    psum x1, blocking collectives, per_device(): mixed = lax.psum(partial_value.astype(jnp.bfloat16), 'tp')  10.7 us
    ppermute x3, waiting for transfers between devices, per_device(): long_array = lax.ppermute(long_array, 'kv', aux)  9.49 us
    pmax x1, blocking collectives, per_device(): block_max = lax.pmax(local_max, 'kv')  8.5 us
    unnamed x29, local copies, waits for them, and re-layouts  5.34 us
    ppermute x3, starting transfers between devices, per_device(): long_array = lax.ppermute(long_array, 'kv', aux)  3.11 us
    dot_general x1, matrix products, per_device(): lax.dot_general(attended, w_out, (((1,), (1,)), ((), ())), preferred_elem...  2.23 us
  transfers between devices with their start and end apart: 3, of which 2 were waited for; matrix products, arithmetic and copies ran while one was open for 7% of the time, Pallas kernels for 0%

profile of v1, /device:TPU:0, one launch (start us, length us, event | category | flops | bytes accessed | tf_op | source)
XLA Modules:
  0.0 85.9 jit_solution(7290227401450269527)
XLA Ops:
  0.6 3.1 %collective-permute-start = (bf16[8,1024]{1,0:T(8,128)(2,1)}, bf16[8,1024]{1,0:T(8,128)(2,1)S(1)}, u32[]{:S(2)}, u32[]{:S(2)}) collective-permute-start(bf16[8,1024]{1,0:T(8,128)(2,1)} %param.13), channel_id=1, source_target_pairs={{0,4},{4,8},{8,12},{12,0},{1,5},{5,9},{9,13},{13,1},{2,6},{6,10},{... | collective-permute-start | bytes 49160 | tf_op jit(solution)/shard_map/ppermute | solution.py:40
  3.8 4.0 %collective-permute-done = bf16[8,1024]{1,0:T(8,128)(2,1)S(1)} collective-permute-done((bf16[8,1024]{1,0:T(8,128)(2,1)}, bf16[8,1024]{1,0:T(8,128)(2,1)S(1)}, u32[]{:S(2)}, u32[]{:S(2)}) %collective-permute-start) | collective-permute-done | bytes 16416 | tf_op jit(solution)/shard_map/ppermute | solution.py:40
  7.7 5.5 %collective-permute-done.1 = bf16[8,1024]{1,0:T(8,128)(2,1)S(1)} collective-permute-done((bf16[8,1024]{1,0:T(8,128)(2,1)S(1)}, bf16[8,1024]{1,0:T(8,128)(2,1)S(1)}, u32[]{:S(2)}, u32[]{:S(2)}) %collective-permute-start.1) | collective-permute-done | bytes 16416 | tf_op jit(solution)/shard_map/ppermute | solution.py:40
  13.2 0.7 broadcast_compare_fusion
  14.0 2.6 %copy.18 = bf16[8,768,128]{1,2,0:T(8,128)(2,1)} copy(bf16[8,768,128]{2,1,0:T(8,128)(2,1)} %param.21) | data formatting | bytes 3145728 | tf_op args[8]
  16.6 2.7 %copy.19 = bf16[8,768,128]{1,2,0:T(8,128)(2,1)} copy(bf16[8,768,128]{2,1,0:T(8,128)(2,1)} %param.22) | data formatting | bytes 3145728 | tf_op args[9]
  19.4 0.2 fusion.9
  19.6 0.1 fusion.11
  19.7 0.2 fusion.15
  19.9 0.1 fusion.13
  20.0 0.4 fusion.17
  20.4 19.5 %psum.42 = bf16[8,1024]{1,0:T(8,128)(2,1)S(1)} all-reduce(f32[8,1024]{1,0:T(8,128)S(1)} %fusion.17), channel_id=1, replica_groups=mesh['grp'=2,'kv'=4,'tp'=4] {'kv'}, use_global_device_ids=true, to_apply=%region_1.2 | all-reduce | flops 8192 | bytes 49152 | tf_op jit(solution)/shard_map/psum | solution.py:57
  39.9 0.1 reshape.76
  40.0 1.1 %fusion.22 = f32[8,16]{1,0:T(8,128)S(1)} fusion(f32[8,16]{1,0:T(8,128)S(1)} %copy-done.6, bf16[8,4096]{1,0:T(8,128)(2,1)S(1)} %fusion.11, bf16[4096,64]{0,1:T(8,128)(2,1)} %param.18, s32[]{:T(128)S(6)} %select_n.35, f32[16]{0:T(128)S(1)} %dynamic_slice.16), kind=kOutput, calls=%fused_computation.43 | convolution fusion | flops 1049856 | bytes 197700 | tf_op jit(solution)/shard_map/dot_general | solution.py:64
  41.1 1.8 %fusion.33 = (f32[8,2,8]{2,1,0:T(2,128)S(1)}, f32[8,2,8,768]{3,2,1,0:T(8,128)S(1)}) fusion(f32[8,16,768]{2,1,0:T(8,128)S(1)} %copy-done.1, f32[8,16]{1,0:T(8,128)S(1)} %fusion.22, bf16[8,2,8,64]{3,2,1,0:T(8,128)(2,1)S(1)} %reshape.76, bf16[8,768,2,64]{1,3,2,0:T(8,128)(2,1)} %bitcast.24, pred[8,768]{1,0:T(8,128)(4,1)S(1)} %broadcast_compare_fusion), kind=kOutput, calls=%fused_computation.52 | convolution fusion | flops 13074304 | bytes 2382848 | tf_op jit(solution)/shard_map/skgd,spkd->skgp/dot_general | solution.py:71
  42.9 8.5 %pmax.7 = f32[8,2,8]{2,1,0:T(2,128)S(1)} all-reduce(f32[8,2,8]{2,1,0:T(2,128)S(1)} %get-tuple-element.12), channel_id=1, replica_groups=mesh['grp'=2,'kv'=4,'tp'=4] {'kv'}, use_global_device_ids=true, to_apply=%region_3.4 | all-reduce | flops 128 | bytes 1024 | tf_op jit(solution)/shard_map/pmax | solution.py:91
  51.4 0.2 fusion.3
  51.7 2.0 %convolution_multiply_fusion.1 = f32[8,2,8,64]{3,2,1,0:T(8,128)S(1)} fusion(bf16[8,768,2,64]{1,3,2,0:T(8,128)(2,1)} %bitcast.25, f32[8,2,8,768]{3,2,1,0:T(8,128)S(1)} %get-tuple-element.13, f32[8,2,8]{2,1,0:T(2,128)S(1)} %get-tuple-element.12, pred[8,768]{1,0:T(8,128)(4,1)S(1)} %broadcast_compare_fusion, f32[8,2,8]{2,1,0:T(2,128)S(1)} %bitcast.30), kind=kOutput, calls=%fused_computation.3 | convolution fusion | flops 12886016 | bytes 2006016 | tf_op jit(solution)/shard_map/skgp,spkd->skgd/dot_general | solution.py:85
  53.7 18.7 %all-reduce = (f32[8,2,8,64]{3,2,1,0:T(8,128)S(1)}, bf16[8,128]{1,0:T(8,128)(2,1)S(1)}, f32[8,2,8]{2,1,0:T(2,128)S(1)}, bf16[8,128]{1,0:T(8,128)(2,1)S(1)}) all-reduce(f32[8,2,8,64]{3,2,1,0:T(8,128)S(1)} %convolution_multiply_fusion.1, f32[8,128]{1,0:T(8,128)S(1)} %fusion.15, ...), channel_id=1, replica_groups=mesh['grp'=2,'kv'=4,'tp'=4] {'kv'}, use_global_device_ids=true, to_apply=%region_4.5 | all-reduce | flops 10368 | bytes 78848 | tf_op jit(solution)/shard_map/psum | solution.py:93
  72.5 0.1 fusion.34
  72.7 0.1 divide_convert_fusion
  72.9 0.1 convert_element_type.49
  73.0 2.2 %convolution_convert_fusion = bf16[8,1024]{1,0:T(8,128)(2,1)S(1)} fusion(bf16[8,1024]{1,0:T(8,128)(2,1)S(1)} %convert_element_type.49, bf16[1024,1024]{1,0:T(8,128)(2,1)} %param.20), kind=kOutput, calls=%fused_computation.4 | convolution fusion | flops 16785408 | bytes 2129920 | tf_op jit(solution)/shard_map/dot_general | solution.py:114
  75.2 10.7 %psum.47 = bf16[8,1024]{1,0:T(8,128)(2,1)} all-reduce(bf16[8,1024]{1,0:T(8,128)(2,1)S(1)} %convolution_convert_fusion), channel_id=1, replica_groups=mesh['grp'=2,'kv'=4,'tp'=4] {'tp'}, use_global_device_ids=true, to_apply=%region_9.10 | all-reduce | flops 8192 | bytes 32768 | tf_op jit(solution)/shard_map/psum | solution.py:118
  (38 shorter events, 0.4 us)
Async XLA Ops:
  0.6 19.4 %copy-start = (bf16[1024,1024]{1,0:T(8,128)(2,1)S(1)}, bf16[1024,1024]{1,0:T(8,128)(2,1)}, u32[]{:S(2)}) copy-start(bf16[1024,1024]{1,0:T(8,128)(2,1)} %param.15) | copy-start | bytes 6291460
  0.6 7.1 %collective-permute-start = (bf16[8,1024]{1,0:T(8,128)(2,1)}, bf16[8,1024]{1,0:T(8,128)(2,1)S(1)}, u32[]{:S(2)}, u32[]{:S(2)}) collective-permute-start(bf16[8,1024]{1,0:T(8,128)(2,1)} %param.13), channel_id=1, source_target_pairs={{0,4},{4,8},{8,12},{12,0},{1,5},{5,9},{9,13},{13,1},{2,6},{6,10},{... | collective-permute-start | bytes 49160 | tf_op jit(solution)/shard_map/ppermute | solution.py:40
  7.7 5.5 %collective-permute-start.1 = (bf16[8,1024]{1,0:T(8,128)(2,1)S(1)}, bf16[8,1024]{1,0:T(8,128)(2,1)S(1)}, u32[]{:S(2)}, u32[]{:S(2)}) collective-permute-start(bf16[8,1024]{1,0:T(8,128)(2,1)S(1)} %collective-permute-done), channel_id=1, source_target_pairs={{0,4},{4,8},{8,12},{12,0},{1,5},{5,9},{9,13},{13,1},{2,6},{6,10},{... | collective-permute-start | bytes 49160 | tf_op jit(solution)/shard_map/ppermute | solution.py:40
  13.2 6.1 %collective-permute-start.2 = (bf16[8,1024]{1,0:T(8,128)(2,1)S(1)}, bf16[8,1024]{1,0:T(8,128)(2,1)S(1)}, u32[]{:S(2)}, u32[]{:S(2)}) collective-permute-start(bf16[8,1024]{1,0:T(8,128)(2,1)S(1)} %collective-permute-done.1), channel_id=1, source_target_pairs={{0,4},{4,8},{8,12},{12,0},{1,5},{5,9},{9,13},{13,1},{2,6},{6,10},{... | collective-permute-start | bytes 49160 | tf_op jit(solution)/shard_map/ppermute | solution.py:40
  16.6 2.7 %copy-start.9 = (f32[64]{0:T(128)S(1)}, f32[64]{0:T(128)}, u32[]{:S(2)}) copy-start(f32[64]{0:T(128)} %param.19) | copy-start | bytes 772
  16.6 2.8 %copy-start.4 = (bf16[8,1024]{1,0:T(8,128)(2,1)S(1)}, bf16[8,1024]{1,0:T(8,128)(2,1)}, u32[]{:S(2)}) copy-start(bf16[8,1024]{1,0:T(8,128)(2,1)} %param.13) | copy-start | bytes 49156
  16.6 3.0 %copy-start.5 = (f32[4096]{0:T(1024)S(1)}, f32[4096]{0:T(1024)}, u32[]{:S(2)}) copy-start(f32[4096]{0:T(1024)} %param.14) | copy-start | bytes 49156
  16.6 3.1 %copy-start.2 = (bf16[1024,128]{1,0:T(8,128)(2,1)S(1)}, bf16[1024,128]{1,0:T(8,128)(2,1)}, u32[]{:S(2)}) copy-start(bf16[1024,128]{1,0:T(8,128)(2,1)} %param.16) | copy-start | bytes 786436
  16.6 3.3 %copy-start.3 = (bf16[1024,128]{1,0:T(8,128)(2,1)S(1)}, bf16[1024,128]{1,0:T(8,128)(2,1)}, u32[]{:S(2)}) copy-start(bf16[1024,128]{1,0:T(8,128)(2,1)} %param.17) | copy-start | bytes 786436
  19.4 20.6 %copy-start.6 = (f32[8,16]{1,0:T(8,128)S(1)}, f32[8,16]{1,0:T(8,128)}, u32[]{:S(2)}) copy-start(f32[8,16]{1,0:T(8,128)} %param.24) | copy-start | bytes 1540
  19.6 21.5 %copy-start.1 = (f32[8,16,768]{2,1,0:T(8,128)S(1)}, f32[8,16,768]{2,1,0:T(8,128)}, u32[]{:S(2)}) copy-start(f32[8,16,768]{2,1,0:T(8,128)} %param.23) | copy-start | bytes 1179652
  72.4 13.5 %copy-start.7 = (bf16[8,128]{1,0:T(8,128)(2,1)}, bf16[8,128]{1,0:T(8,128)(2,1)S(1)}, u32[]{:S(2)}) copy-start(bf16[8,128]{1,0:T(8,128)(2,1)S(1)} %get-tuple-element.4) | copy-start | bytes 6148
  72.4 13.5 %copy-start.8 = (bf16[8,128]{1,0:T(8,128)(2,1)}, bf16[8,128]{1,0:T(8,128)(2,1)S(1)}, u32[]{:S(2)}) copy-start(bf16[8,128]{1,0:T(8,128)(2,1)S(1)} %get-tuple-element.6) | copy-start | bytes 6148
